TPU v7x, 32 devices: a whole 2x2x4 slice. The times are simulated.
32 devices in a mesh: ep: 8 (over z, x), tp: 4 (over y, core).
Axes of the slice: x: 2, y: 2, z: 4, core: 2. Of those that a mesh axis runs over, the one named last changes fastest.
Arguments:
- queries: bfloat16 [4096, 2048], P('ep', 'tp'), may hold values from -6 to 6
- keys: bfloat16 [4096, 2048], P('ep', 'tp'), may hold values from -12 to 12
- values: bfloat16 [4096, 2048], P('ep', 'tp'), may hold values from -8 to 8
- key_bias: bfloat16 [4096, 16], P('ep', 'tp'), may hold values from -16 to 0
- out_weight: bfloat16 [2048, 2048], P('tp'), may hold values from -0.1875 to 0.1875
- moe_input: bfloat16 [1024, 2048], P('ep'), may hold values from -6 to 6
- moe_gain: float32 [2048], replicated, may hold values from 0.1 to 1.9
- route_ids: int32 [1024, 2], P('ep'), may hold values from 0 to 7, all different within a row; in each aligned block of 128 rows (0 to 127, 128 to 255, ...) at most 48 rows name the same one
- route_scores: float32 [1024, 2], P('ep'), may hold values from 0.05 to 1
- shared_gate: bfloat16 [2048, 2048], P(None, 'tp'), may hold values from -0.125 to 0.125
- shared_up: bfloat16 [2048, 2048], P(None, 'tp'), may hold values from -0.125 to 0.125
- shared_down: bfloat16 [2048, 2048], P('tp'), may hold values from -0.1875 to 0.1875
- expert_gate: bfloat16 [8, 2048, 2048], P('ep', None, 'tp'), may hold values from -0.125 to 0.125
- expert_up: bfloat16 [8, 2048, 2048], P('ep', None, 'tp'), may hold values from -0.125 to 0.125
- expert_down: bfloat16 [8, 2048, 2048], P('ep', 'tp'), may hold values from -0.1875 to 0.1875
Outputs:
- mixed_tokens: bfloat16 [4096, 2048], P('ep', 'tp')
- expert_mix: bfloat16 [1024, 2048], P('ep', 'tp')
Inputs may be any that keep to these rules, and one draw needn't show every extreme that they name: `route_ids`: each row names 2 different experts. Among the 128 rows of one index of ep no expert is named by more than 48 rows, and in some such block one expert is named by exactly 48 rows.
All inputs are finite; a program needn't handle non-finite values.
Results may differ from a plain program's by a relative error of at most 0.019.
Values may be sent and summed in bfloat16 or wider, within the bound.
A program may use at most 128 MiB of HBM per device.

v0:
```python
import functools

import jax
import jax.numpy as jnp
from jax import lax
from jax.experimental import pallas as pl
from jax.experimental.pallas import tpu as pltpu
from jax.sharding import PartitionSpec as P

EPS_NORM = 1e-06
ROUTED_SCALE = 2.5
LOG2E = 1.4426950408889634
BIAS_ROWS = 16
MESH = pl.DeviceIdType.MESH


def attention_kernel(
    tp_count,
    query_ref,
    key_ref,
    value_ref,
    bias_ref,
    tri_ref,
    partial_ref,
    out_ref,
    partial_out,
    local_sem,
    send_sem,
    recv_sem,
):
    block = pl.program_id(0)
    own_tp = lax.axis_index("tp")
    width_out = partial_out.shape[2]
    local = pltpu.make_async_copy(
        partial_ref.at[:, columns(own_tp, width_out)], partial_out.at[own_tp], local_sem.at[0]
    )

    def piece(i, arriving):
        other = lax.rem(own_tp + i, tp_count)
        return pltpu.make_async_remote_copy(
            src_ref=partial_ref.at[:, columns(other, width_out)],
            dst_ref=partial_out.at[other if arriving else own_tp],
            send_sem=send_sem.at[other],
            recv_sem=recv_sem.at[other if arriving else own_tp],
            device_id={"tp": other},
            device_id_type=MESH,
        )

    @pl.when(block == 0)
    def _():
        barrier = pltpu.get_barrier_semaphore()
        for i in range(1, tp_count):
            pl.semaphore_signal(
                barrier,
                inc=1,
                device_id={"tp": lax.rem(own_tp + i, tp_count)},
                device_id_type=MESH,
            )
        pl.semaphore_wait(barrier, tp_count - 1)
        for i in range(1, tp_count):
            piece(i, False).start()
        local.start()

    share, size = query_ref.shape[1:]
    span = key_ref.shape[1]
    groups = span // share
    offset = lax.rem(lax.axis_index("ep"), groups) * share
    width = tri_ref.shape[0]
    query = query_ref[block]
    scale = size ** (-0.5) * LOG2E

    def unit(key_block, carry, masked):
        total, passed = carry
        key = key_ref[key_block]
        value = value_ref[key_block]
        bias = bias_ref[key_block].astype(jnp.float32) * LOG2E
        for start in range(span - width, -1, -width):
            row = jnp.concatenate(
                [bias[i : i + 1, :] for i in range(start // size, (start + width) // size)],
                axis=1,
            )
            logit = (
                lax.dot_general(
                    query,
                    key[start : start + width],
                    (((1,), (1,)), ((), ())),
                    preferred_element_type=jnp.float32,
                )
                * scale
                + row
            )
            drop = jnp.maximum(logit, jnp.log(1.0 + jnp.exp2(jnp.minimum(logit, 126.0))) * LOG2E)
            base = logit - drop
            if masked:
                shape = (share, width)
                visible = start + lax.broadcasted_iota(
                    jnp.int32, shape, 1
                ) < offset + lax.broadcasted_iota(jnp.int32, shape, 0)
                drop = jnp.where(visible, drop, 0.0)
            later = jnp.dot(
                drop.astype(jnp.bfloat16), tri_ref[...], preferred_element_type=jnp.float32
            )
            weight = jnp.exp2(base - later - passed)
            if masked:
                weight = jnp.where(visible, weight, 0.0)
            passed = passed + later[:, 0:1] + drop[:, 0:1]
            total = total + jnp.dot(
                weight.astype(jnp.bfloat16),
                value[start : start + width],
                preferred_element_type=jnp.float32,
            )
        return (total, passed)

    carry = (jnp.zeros((share, size), jnp.float32), jnp.zeros((share, 1), jnp.float32))
    carry = unit(block, carry, True)
    carry = lax.fori_loop(0, block, lambda i, c: unit(block - 1 - i, c, False), carry)
    out_ref[0] = carry[0].astype(out_ref.dtype)

    @pl.when(block == pl.num_programs(0) - 1)
    def _():
        local.wait()
        for i in range(1, tp_count):
            piece(i, True).wait_recv()
        for i in range(1, tp_count):
            piece(i, False).wait_send()


def attention(query, key, value, bias, partial, tp_count):
    blocks, share, size = query.shape
    span = key.shape[1]
    width = min(256, span)
    index = jnp.arange(width)
    tri = (index[:, None] > index[None, :]).astype(jnp.bfloat16)
    dma = pltpu.SemaphoreType.DMA
    work = blocks * (blocks + 1) // 2 * share * span
    whole = pl.BlockSpec(memory_space=pltpu.VMEM)
    return pl.pallas_call(
        functools.partial(attention_kernel, tp_count),
        grid=(blocks,),
        in_specs=[whole] * 6,
        out_specs=[
            pl.BlockSpec((1, share, size), lambda i: (i, 0, 0)),
            pl.BlockSpec(memory_space=pl.ANY),
        ],
        out_shape=[
            jax.ShapeDtypeStruct((blocks, share, size), jnp.bfloat16),
            jax.ShapeDtypeStruct(
                (tp_count, partial.shape[0], partial.shape[1] // tp_count), jnp.bfloat16
            ),
        ],
        scratch_shapes=[dma((1,)), dma((tp_count,)), dma((tp_count,))],
        cost_estimate=pl.CostEstimate(
            flops=work * (4 * size + 2 * width),
            bytes_accessed=key.size * 5,
            transcendentals=3 * work,
        ),
        compiler_params=pltpu.CompilerParams(
            dimension_semantics=("arbitrary",),
            vmem_limit_bytes=40 * 1024 * 1024,
            collective_id=2,
            has_side_effects=True,
        ),
        name="stick",
    )(query, key, value, bias, tri, partial)


def others_across(own_tp, tp_count):
    pair = 2 - tp_count % 2
    chips = tp_count // pair
    return [
        lax.rem(own_tp // pair + i, chips) * pair + lax.rem(own_tp, pair) for i in range(1, chips)
    ]


def beside(own_tp, tp_count):
    if tp_count % 2:
        return []
    return [own_tp + 1 - 2 * lax.rem(own_tp, 2)]


def near_first(own_tp, tp_count):
    return others_across(own_tp, tp_count) + beside(own_tp, tp_count)


def columns(index, width):
    return pl.ds(pl.multiple_of(index * width, width), width)


def meet(ep_count, tp_count):
    own_ep, own_tp = lax.axis_index("ep"), lax.axis_index("tp")
    barrier = pltpu.get_barrier_semaphore()
    for i in range(1, ep_count):
        pl.semaphore_signal(
            barrier, inc=1, device_id={"ep": lax.rem(own_ep + i, ep_count)}, device_id_type=MESH
        )
    for i in range(1, tp_count):
        pl.semaphore_signal(
            barrier, inc=1, device_id={"tp": lax.rem(own_tp + i, tp_count)}, device_id_type=MESH
        )
    pl.semaphore_wait(barrier, ep_count + tp_count - 2)


def exchange_kernel(
    counts,
    query_ref,
    key_ref,
    value_ref,
    bias_ref,
    rows_ref,
    weight_ref,
    query_out,
    key_out,
    value_out,
    bias_out,
    rows_out,
    weight_out,
    local_sem,
    query_send,
    query_recv,
    part_send,
    part_recv,
    rows_send,
    rows_recv,
    relay_send,
    relay_recv,
    pass_send,
    weight_send,
    weight_recv,
):
    ep_count, tp_count, heads = counts
    groups = ep_count // heads
    share, size = query_out.shape[1:]
    depth = weight_ref.shape[0]
    col_count = weight_out.shape[1]
    own, own_tp = lax.axis_index("ep"), lax.axis_index("tp")
    own_head, own_group = own // groups, lax.rem(own, groups)
    rows_own = rows_out.at[:, :, columns(own_tp, col_count)]

    def query_part(device):
        return query_ref.at[columns(lax.rem(device, groups), share), columns(device // groups, size)]

    def part(kind, head):
        if kind == 2:
            return bias_ref.at[head]
        return (key_ref, value_ref)[kind].at[:, columns(head, size)]

    part_outs = (key_out, value_out, bias_out)

    def remote(source, target, send, recv, axis, device):
        return pltpu.make_async_remote_copy(
            src_ref=source,
            dst_ref=target,
            send_sem=send,
            recv_sem=recv,
            device_id={axis: device},
            device_id_type=MESH,
        )

    meet(ep_count, tp_count)
    sent = []

    def start(copy):
        copy.start()
        sent.append(copy)

    local = [
        pltpu.make_async_copy(rows_ref.at[own], rows_out.at[own, :, columns(own_tp, col_count)], local_sem.at[0]),
        pltpu.make_async_copy(query_part(own), query_out.at[own], local_sem.at[1]),
        pltpu.make_async_copy(
            weight_ref.at[:, columns(own_tp, col_count)],
            weight_out.at[columns(own_tp, depth), :],
            local_sem.at[2],
        ),
    ] + [
        pltpu.make_async_copy(part(kind, own_head), part_outs[kind].at[own], local_sem.at[3 + kind])
        for kind in range(3)
    ]
    for copy in local:
        copy.start()
    for i in range(1, ep_count):
        other = lax.rem(own + i, ep_count)
        start(
            remote(
                rows_ref.at[other],
                rows_out.at[own, :, columns(own_tp, col_count)],
                rows_send.at[other],
                rows_recv.at[own],
                "ep",
                other,
            )
        )
    for step in range(1, groups):
        group = lax.rem(own_group + step, groups)
        other = own_head * groups + group
        for kind in range(3):
            start(
                remote(
                    part(kind, own_head),
                    part_outs[kind].at[own],
                    part_send.at[kind, other],
                    part_recv.at[kind, own],
                    "ep",
                    other,
                )
            )
    for i in range(1, heads):
        head = lax.rem(own_head + i, heads)
        other = head * groups + own_group
        for kind in range(3):
            start(
                remote(
                    part(kind, head),
                    part_outs[kind].at[own],
                    part_send.at[kind, other],
                    part_recv.at[kind, own],
                    "ep",
                    other,
                )
            )
    for i in range(1, ep_count):
        other = lax.rem(own + i, ep_count)
        start(
            remote(
                query_part(other),
                query_out.at[own],
                query_send.at[other],
                query_recv.at[own],
                "ep",
                other,
            )
        )
    for i in range(1, ep_count):
        other = lax.rem(own + i, ep_count)
        remote(
            rows_ref.at[other],
            rows_out.at[other, :, columns(own_tp, col_count)],
            rows_send.at[other],
            rows_recv.at[other],
            "ep",
            other,
        ).wait_recv()
    local[0].wait()
    for other in near_first(own_tp, tp_count):
        start(remote(rows_own, rows_own, relay_send.at[other], relay_recv.at[own_tp], "tp", other))
    for i in range(1, tp_count):
        other = lax.rem(own_tp + i, tp_count)
        start(
            remote(
                weight_ref.at[:, columns(other, col_count)],
                weight_out.at[columns(own_tp, depth), :],
                weight_send.at[other],
                weight_recv.at[own_tp],
                "tp",
                other,
            )
        )

    def part_arrival(kind, source):
        target = part_outs[kind].at[source]
        remote(
            target, target, part_send.at[kind, source], part_recv.at[kind, source], "ep", source
        ).wait_recv()

    for i in range(1, heads):
        source = lax.rem(own_head + heads - i, heads) * groups + own_group
        for kind in range(3):
            part_arrival(kind, source)
            for step in range(1, groups):
                group = lax.rem(own_group + step, groups)
                target = part_outs[kind].at[source]
                start(
                    remote(
                        target,
                        target,
                        part_send.at[kind, source - own_group + group],
                        part_recv.at[kind, source],
                        "ep",
                        own_head * groups + group,
                    )
                )
    def rows_arrival(slot):
        arrived = rows_out.at[:, :, columns(slot, col_count)]
        remote(
            arrived, arrived, relay_send.at[slot], relay_recv.at[slot], "tp", slot
        ).wait_recv()
        return arrived

    for slot in others_across(own_tp, tp_count):
        arrived = rows_arrival(slot)
        for other in beside(own_tp, tp_count):
            start(
                remote(arrived, arrived, pass_send.at[slot], relay_recv.at[slot], "tp", other)
            )
    for i in range(heads):
        for step in range(1, groups):
            group = lax.rem(own_group + step, groups)
            source = lax.rem(own_head + heads - i, heads) * groups + group
            for kind in range(3):
                part_arrival(kind, source)
    for i in range(1, ep_count):
        other = lax.rem(own + i, ep_count)
        remote(
            query_part(other),
            query_out.at[other],
            query_send.at[other],
            query_recv.at[other],
            "ep",
            other,
        ).wait_recv()
    for i in range(1, tp_count):
        other = lax.rem(own_tp + i, tp_count)
        target = weight_out.at[columns(other, depth), :]
        remote(
            target, target, weight_send.at[other], weight_recv.at[other], "tp", other
        ).wait_recv()
    for other in beside(own_tp, tp_count):
        rows_arrival(other)
        for slot in others_across(other, tp_count):
            rows_arrival(slot)
    for copy in sent:
        copy.wait_send()
    for copy in local[1:]:
        copy.wait()


def exchange(queries, keys, values, bias, rows, weight, counts):
    ep_count, tp_count, heads = counts
    span = queries.shape[0]
    size = queries.shape[1] // heads
    share = span * heads // ep_count
    depth, features = weight.shape
    whole = pl.BlockSpec(memory_space=pltpu.VMEM)
    free = pl.BlockSpec(memory_space=pl.ANY)
    dma = pltpu.SemaphoreType.DMA
    kind = jnp.bfloat16
    return pl.pallas_call(
        functools.partial(exchange_kernel, counts),
        in_specs=[whole] * 6,
        out_specs=[free] * 6,
        out_shape=[
            jax.ShapeDtypeStruct((ep_count, share, size), kind),
            jax.ShapeDtypeStruct((ep_count, span, size), kind),
            jax.ShapeDtypeStruct((ep_count, span, size), kind),
            jax.ShapeDtypeStruct((ep_count,) + bias.shape[1:], kind),
            jax.ShapeDtypeStruct((ep_count, rows.shape[1], features), kind),
            jax.ShapeDtypeStruct((depth * tp_count, features // tp_count), kind),
        ],
        scratch_shapes=[
            dma((6,)),
            dma((ep_count,)),
            dma((ep_count,)),
            dma((3, ep_count)),
            dma((3, ep_count)),
            dma((ep_count,)),
            dma((ep_count,)),
            dma((tp_count,)),
            dma((tp_count,)),
            dma((tp_count,)),
            dma((tp_count,)),
            dma((tp_count,)),
        ],
        compiler_params=pltpu.CompilerParams(
            collective_id=0, has_side_effects=True, vmem_limit_bytes=40 * 1024 * 1024
        ),
        name="exchange",
    )(queries, keys, values, bias, rows, weight)


def gather_kernel(
    counts,
    part_ref,
    back_ref,
    out_ref,
    back_out,
    local_sem,
    send_sem,
    recv_sem,
    relay_send,
    relay_recv,
    pass_send,
    back_send,
    back_recv,
):
    ep_count, tp_count, heads = counts
    groups = ep_count // heads
    share, size = part_ref.shape[1:]
    own, own_tp = lax.axis_index("ep"), lax.axis_index("tp")

    def place_of(source, slot):
        return out_ref.at[
            columns(lax.rem(source, groups), share), columns(slot * heads + source // groups, size)
        ]

    def remote(source, target, send, recv, axis, device):
        return pltpu.make_async_remote_copy(
            src_ref=source,
            dst_ref=target,
            send_sem=send,
            recv_sem=recv,
            device_id={axis: device},
            device_id_type=MESH,
        )

    meet(ep_count, tp_count)
    local = pltpu.make_async_copy(part_ref.at[own], place_of(own, own_tp), local_sem.at[0])
    local.start()
    local_back = pltpu.make_async_copy(back_ref.at[own], back_out.at[own], local_sem.at[1])
    local_back.start()
    sent = []

    def start(copy):
        copy.start()
        sent.append(copy)

    for i in range(1, ep_count):
        other = lax.rem(own + i, ep_count)
        start(
            remote(
                part_ref.at[other],
                place_of(own, own_tp),
                send_sem.at[other],
                recv_sem.at[own],
                "ep",
                other,
            )
        )
    for i in range(1, ep_count):
        other = lax.rem(own + i, ep_count)
        start(
            remote(
                back_ref.at[other],
                back_out.at[own],
                back_send.at[other],
                back_recv.at[own],
                "ep",
                other,
            )
        )
    sources = [lax.rem(own + ep_count - i, ep_count) for i in range(ep_count)]
    for i, source in enumerate(sources):
        piece = place_of(source, own_tp)
        if i == 0:
            local.wait()
        else:
            remote(
                piece, piece, send_sem.at[source], recv_sem.at[source], "ep", source
            ).wait_recv()
        for other in near_first(own_tp, tp_count):
            start(
                remote(
                    piece,
                    piece,
                    relay_send.at[source, other],
                    relay_recv.at[source, own_tp],
                    "tp",
                    other,
                )
            )

    def arrival(source, slot):
        piece = place_of(source, slot)
        remote(
            piece, piece, relay_send.at[source, slot], relay_recv.at[source, slot], "tp", slot
        ).wait_recv()
        return piece

    for source in sources:
        for slot in others_across(own_tp, tp_count):
            piece = arrival(source, slot)
            for other in beside(own_tp, tp_count):
                start(
                    remote(
                        piece,
                        piece,
                        pass_send.at[source, slot],
                        relay_recv.at[source, slot],
                        "tp",
                        other,
                    )
                )
    for source in sources:
        for other in beside(own_tp, tp_count):
            arrival(source, other)
            for slot in others_across(other, tp_count):
                arrival(source, slot)
    for source in sources[1:]:
        remote(
            back_ref.at[source],
            back_out.at[source],
            back_send.at[source],
            back_recv.at[source],
            "ep",
            source,
        ).wait_recv()
    for copy in sent:
        copy.wait_send()
    local_back.wait()


def gather(parts, back, counts):
    ep_count, tp_count, heads = counts
    _, share, size = parts.shape
    dma = pltpu.SemaphoreType.DMA
    return pl.pallas_call(
        functools.partial(gather_kernel, counts),
        in_specs=[pl.BlockSpec(memory_space=pltpu.VMEM)] * 2,
        out_specs=[pl.BlockSpec(memory_space=pl.ANY)] * 2,
        out_shape=[
            jax.ShapeDtypeStruct(
                (share * ep_count // heads, tp_count * heads * size), jnp.bfloat16
            ),
            jax.ShapeDtypeStruct(back.shape, jnp.bfloat16),
        ],
        scratch_shapes=[
            dma((2,)),
            dma((ep_count,)),
            dma((ep_count,)),
            dma((ep_count, tp_count)),
            dma((ep_count, tp_count)),
            dma((ep_count, tp_count)),
            dma((ep_count,)),
            dma((ep_count,)),
        ],
        compiler_params=pltpu.CompilerParams(collective_id=1, has_side_effects=True),
        cost_estimate=pl.CostEstimate(
            flops=0, bytes_accessed=parts.size * 100, transcendentals=0
        ),
        name="gather",
    )(parts, back)


def body(
    queries,
    keys,
    values,
    key_bias,
    out_weight,
    moe_input,
    moe_gain,
    route_ids,
    route_scores,
    shared_gate,
    shared_up,
    shared_down,
    expert_gate,
    expert_up,
    expert_down,
):
    span = queries.shape[0]
    heads = key_bias.shape[1]
    size = queries.shape[1] // heads
    ep_count = lax.axis_size("ep")
    tp_count = lax.axis_size("tp")

    counts = (ep_count, tp_count, heads)
    col_count = out_weight.shape[1] // tp_count
    bias_parts = key_bias.T.reshape(heads, span // size, size)
    bias_parts = jnp.pad(bias_parts, ((0, 0), (0, BIAS_ROWS - span // size), (0, 0)))

    token_count = moe_input.shape[0]
    inputs = moe_input.astype(jnp.float32)
    normed = (
        inputs * lax.rsqrt(jnp.mean(inputs * inputs, axis=-1, keepdims=True) + EPS_NORM) * moe_gain
    ).astype(jnp.bfloat16)
    own_cols = lax.dynamic_slice_in_dim(normed, lax.axis_index("tp") * col_count, col_count, 1)
    shared_hidden = (
        jax.nn.silu(jnp.dot(normed, shared_gate, preferred_element_type=jnp.float32))
        * jnp.dot(normed, shared_up, preferred_element_type=jnp.float32)
    ).astype(jnp.bfloat16)
    local_experts = expert_gate.shape[0]
    expert_count = local_experts * ep_count
    topk = route_ids.shape[1]
    capacity = 3 * token_count * topk // (2 * expert_count)
    send_slots = expert_count * capacity
    onehot = route_ids[:, :, None] == jnp.arange(expert_count, dtype=jnp.int32)
    named = jnp.sum(onehot.astype(jnp.bfloat16), axis=1)
    row = jnp.arange(token_count)
    earlier = jnp.dot(
        (row[:, None] > row[None, :]).astype(jnp.bfloat16),
        named,
        preferred_element_type=jnp.float32,
    ).astype(jnp.int32)
    place_in = jnp.sum(jnp.where(onehot, earlier[:, None, :], 0), axis=2)
    slot_ids = route_ids * capacity + place_in
    matches = slot_ids[None] == jnp.arange(send_slots, dtype=jnp.int32)[:, None, None]
    dispatch = jnp.sum(matches.astype(jnp.bfloat16), axis=2)
    outgoing = jnp.dot(dispatch, own_cols, preferred_element_type=jnp.float32).astype(jnp.bfloat16)
    query_all, key_all, value_all, bias_all, grid, weight_cols = exchange(
        queries,
        keys,
        values,
        bias_parts,
        outgoing.reshape(ep_count, local_experts * capacity, col_count),
        out_weight,
        counts,
    )
    grid = grid.reshape(ep_count, local_experts, capacity, -1)
    gate_sum = jnp.einsum("secd,edf->secf", grid, expert_gate, preferred_element_type=jnp.float32)
    up_sum = jnp.einsum("secd,edf->secf", grid, expert_up, preferred_element_type=jnp.float32)
    expert_hidden = (jax.nn.silu(gate_sum) * up_sum).astype(jnp.bfloat16)
    routed = jnp.einsum(
        "secf,efd->secd", expert_hidden, expert_down, preferred_element_type=jnp.float32
    ).reshape(send_slots, -1)
    common = jnp.dot(shared_hidden, shared_down, preferred_element_type=jnp.float32)
    partial = jnp.concatenate([routed, common], axis=0).astype(jnp.bfloat16)
    mixed_heads, partial_all = attention(
        query_all, key_all, value_all, bias_all, partial, tp_count
    )
    expert_sum = jnp.sum(partial_all.astype(jnp.float32), axis=0)
    routed_sum = expert_sum[:send_slots].astype(jnp.bfloat16)
    common_sum = expert_sum[send_slots:]
    heads_all, returned = gather(
        mixed_heads, routed_sum.reshape(ep_count, local_experts * capacity, col_count), counts
    )
    returned = returned.reshape(send_slots, col_count)
    mixed_tokens = jnp.dot(heads_all, weight_cols, preferred_element_type=jnp.float32).astype(
        jnp.bfloat16
    )
    gates = route_scores / jnp.sum(route_scores, axis=-1, keepdims=True) * ROUTED_SCALE
    gates_high = gates.astype(jnp.bfloat16)
    gates_low = (gates - gates_high.astype(jnp.float32)).astype(jnp.bfloat16)

    def combined(part):
        table = jnp.sum(jnp.where(matches, part[None], jnp.bfloat16(0)), axis=2)
        return jnp.einsum("st,sd->td", table, returned, preferred_element_type=jnp.float32)

    expert_mix = (common_sum + combined(gates_high) + combined(gates_low)).astype(jnp.bfloat16)
    return (mixed_tokens, expert_mix)


def solution(mesh):
    return jax.shard_map(
        body,
        mesh=mesh,
        in_specs=(
            P("ep", "tp"),
            P("ep", "tp"),
            P("ep", "tp"),
            P("ep", "tp"),
            P("tp", None),
            P("ep", None),
            P(),
            P("ep", None),
            P("ep", None),
            P(None, "tp"),
            P(None, "tp"),
            P("tp", None),
            P("ep", None, "tp"),
            P("ep", None, "tp"),
            P("ep", "tp", None),
        ),
        out_specs=(P("ep", "tp"), P("ep", "tp")),
        check_vma=False,
    )
```

profile of v0, /device:TPU:31, one launch (start us, length us, event | category | flops | bytes accessed | tf_op | source)
XLA Modules:
  0.0 155.7 jit_solution(10733685080055319524)
XLA Ops:
  0.6 0.0 copy-start
  0.6 1.4 fusion.22
  2.0 0.7 reduce_sum.89
  2.7 0.7 subtract_convert_fusion
  3.4 0.7 fusion.48
  4.1 0.1 convolution_convert_fusion.4
  4.2 0.7 select_reduce_fusion
  5.0 0.7 multiply_add_fusion
  5.6 0.7 reshape.56
  6.4 0.7 fusion.44
  7.1 1.2 fusion.24
  8.3 0.0 copy-start.14
  8.4 0.8 copy-done.14
  9.1 2.7 %fusion.52 = f32[128,512]{1,0:T(8,128)} fusion(bf16[128,2048]{1,0:T(8,128)(2,1)S(1)} %fusion.24, bf16[2048,512]{1,0:T(8,128)(2,1)} %param.24), kind=kOutput, calls=%fused_computation.62 | convolution fusion | flops 268435456 | bytes 2883584 | tf_op jit(solution)/shard_map/dot_general | solution.py:667
  11.9 4.2 %convolution_convert_fusion.1 = bf16[128,2048]{1,0:T(8,128)(2,1)} fusion(bf16[512,2048]{1,0:T(8,128)(2,1)} %param.26, bf16[128,2048]{1,0:T(8,128)(2,1)} %copy-done.14, bf16[2048,512]{1,0:T(8,128)(2,1)} %param.25, f32[128,512]{1,0:T(8,128)} %fusion.52), kind=kOutput, calls=%fused_computation.2 | convolution fusion | flops 537526272 | bytes 5505024 | tf_op jit(solution)/shard_map/dot_general | solution.py:704
  16.1 1.1 convolution_convert_fusion.3
  17.3 0.0 copy-done.3
  17.3 0.0 copy-done.4
  17.3 0.0 copy-start.1
  17.3 1.6 %copy-done.1 = bf16[512,2048]{1,0:T(8,128)(2,1)S(1)} copy-done((bf16[512,2048]{1,0:T(8,128)(2,1)S(1)}, bf16[512,2048]{1,0:T(8,128)(2,1)}, u32[]{:S(2)}) %copy-start.1) | copy-done | bytes 2097176
  18.9 1.0 copy-done.5
  19.9 52.8 %exchange.1 = (bf16[8,256,128]{2,1,0:T(8,128)(2,1)S(1)}, bf16[8,512,128]{2,1,0:T(8,128)(2,1)S(1)}, bf16[8,512,128]{2,1,0:T(8,128)(2,1)S(1)}, bf16[8,16,128]{2,1,...) custom-call(bf16[512,512]{1,0:T(8,128)(2,1)S(1)} %copy-done.3, ...), custom_call_target="tpu_custom_call" | custom-call | tf_op jit(solution)/shard_map/exchange/pallas_call | solution.py:436
  72.8 0.0 copy-start.6
  72.8 1.3 copy-done.6
  74.1 1.0 copy-done.8
  75.1 1.0 copy-done.10
  76.1 0.8 copy-done.12
  76.9 1.2 copy-done.7
  78.1 0.0 copy-done.18
  78.1 1.9 %fusion.5 = f32[8,1,48,512]{3,2,0,1:T(8,128)} fusion(bf16[8,48,2048]{2,1,0:T(8,128)(2,1)S(1)} %get-tuple-element.16, bf16[1,2048,512]{2,1,0:T(8,128)(2,1)S(1)} %copy-done.18), kind=kOutput, calls=%fused_computation.11 | convolution fusion | flops 805306368 | bytes 4456448 | tf_op jit(solution)/shard_map/secd,edf->secf/dot_general | solution.py:698
  79.9 0.0 copy-done
  80.0 5.3 %convolution_convert_fusion = bf16[8,48,2048]{2,1,0:T(8,128)(2,1)} fusion(bf16[1,512,2048]{2,1,0:T(8,128)(2,1)S(1)} %copy-done, bf16[8,48,2048]{2,1,0:T(8,128)(2,1)} %copy-done.7, bf16[1,2048,512]{2,1,0:T(8,128)(2,1)} %param.28, f32[8,1,48,512]{3,2,0,1:T(8,128)} %fusion.5), kind=kOutput, calls=%fused_computation.1 | convolution fusion | flops 1612578816 | bytes 8126464 | tf_op jit(solution)/shard_map/secf,efd->secd/dot_general | solution.py:701
  85.3 0.0 copy-done.15
  85.3 1.8 %pad_maximum_fusion.partial_ref = bf16[512,2048]{1,0:T(8,128)(2,1)S(1)} fusion(bf16[128,2048]{1,0:T(8,128)(2,1)S(1)} %copy-done.15, bf16[384,2048]{1,0:T(8,128)(2,1)} %bitcast.78), kind=kLoop, calls=%fused_computation.3 | loop fusion | flops 4194304 | bytes 4194304 | tf_op jit(solution)/shard_map/concatenate | solution.py:705
  87.1 0.0 copy-done.9
  87.1 0.2 copy-done.11
  87.3 0.1 copy-done.13
  87.4 27.9 %stick.1 = (bf16[8,256,128]{2,1,0:T(8,128)(2,1)S(1)}, bf16[4,512,512]{2,1,0:T(8,128)(2,1)S(1)}) custom-call(bf16[8,256,128]{2,1,0:T(8,128)(2,1)S(1)} %copy-done.13, bf16[8,512,128]{2,1,0:T(8,128)(2,1)S(1)} %copy-done.9, bf16[8,512,128]{2,1,0:T(8,128)(2,1)S(1)} %copy-done.11, bf16[8,16,128]{2,1,0:T(8,128)(2,1)S(1)} %get-tuple-element.15.bias_ref, ...), custom_call_target="tpu_custom_call" | custom-call | flops 4831838208 | bytes 2621440 | tf_op jit(solution)/shard_map/stick/pallas_call | solution.py:137
  115.3 0.0 copy-start.2
  115.4 0.3 convert_reduce_fusion
  115.7 0.5 copy-done.2
  116.1 0.8 slice.13
  116.9 33.3 %gather.1 = (bf16[512,2048]{1,0:T(8,128)(2,1)}, bf16[8,48,512]{2,1,0:T(8,128)(2,1)}) custom-call(bf16[8,256,128]{2,1,0:T(8,128)(2,1)} %copy-done.2, bf16[8,48,512]{2,1,0:T(8,128)(2,1)} %bitcast.77), custom_call_target="tpu_custom_call" | custom-call | bytes 26214400 | tf_op jit(solution)/shard_map/gather/pallas_call | solution.py:604
  150.2 0.0 copy-start.17
  150.2 4.3 %convolution_convert_fusion.2 = bf16[512,512]{1,0:T(8,128)(2,1)} fusion(bf16[512,2048]{1,0:T(8,128)(2,1)} %get-tuple-element.19, bf16[2048,512]{1,0:T(8,128)(2,1)} %copy-done.6), kind=kOutput, calls=%fused_computation.13 | convolution fusion | flops 1074003968 | bytes 4718592 | tf_op jit(solution)/shard_map/dot_general | solution.py:716
  154.5 0.0 copy-done.17
  154.5 0.3 convolution_add_fusion.1
  154.8 0.9 fusion.21
  (17 shorter events, 0.1 us)
Async XLA Ops:
  0.6 79.3 %copy-start = (bf16[1,512,2048]{2,1,0:T(8,128)(2,1)S(1)}, bf16[1,512,2048]{2,1,0:T(8,128)(2,1)}, u32[]{:S(2)}) copy-start(bf16[1,512,2048]{2,1,0:T(8,128)(2,1)} %param.29) | copy-start | bytes 6291460
  8.3 0.8 copy-start.14
  11.9 5.4 %copy-start.3 = (bf16[512,512]{1,0:T(8,128)(2,1)S(1)}, bf16[512,512]{1,0:T(8,128)(2,1)}, u32[]{:S(2)}) copy-start(bf16[512,512]{1,0:T(8,128)(2,1)} %query_ref.1) | copy-start | bytes 1572868
  11.9 5.4 %copy-start.4 = (bf16[512,512]{1,0:T(8,128)(2,1)S(1)}, bf16[512,512]{1,0:T(8,128)(2,1)}, u32[]{:S(2)}) copy-start(bf16[512,512]{1,0:T(8,128)(2,1)} %key_ref.1) | copy-start | bytes 1572868
  17.3 1.6 %copy-start.1 = (bf16[512,2048]{1,0:T(8,128)(2,1)S(1)}, bf16[512,2048]{1,0:T(8,128)(2,1)}, u32[]{:S(2)}) copy-start(bf16[512,2048]{1,0:T(8,128)(2,1)} %weight_ref.1) | copy-start | bytes 6291460
  18.9 1.0 copy-start.5
  19.9 58.2 %copy-start.18 = (bf16[1,2048,512]{2,1,0:T(8,128)(2,1)S(1)}, bf16[1,2048,512]{2,1,0:T(8,128)(2,1)}, u32[]{:S(2)}) copy-start(bf16[1,2048,512]{2,1,0:T(8,128)(2,1)} %param.27) | copy-start | bytes 6291460
  72.8 1.3 copy-start.6
  74.1 1.0 copy-start.8
  75.1 1.0 copy-start.10
  76.1 0.8 copy-start.12
  76.9 1.2 copy-start.7
  79.9 5.4 %copy-start.15 = (bf16[128,2048]{1,0:T(8,128)(2,1)S(1)}, bf16[128,2048]{1,0:T(8,128)(2,1)}, u32[]{:S(2)}) copy-start(bf16[128,2048]{1,0:T(8,128)(2,1)} %convolution_convert_fusion.1) | copy-start | bytes 1572868
  85.3 1.8 %copy-start.9 = (bf16[8,512,128]{2,1,0:T(8,128)(2,1)S(1)}, bf16[8,512,128]{2,1,0:T(8,128)(2,1)}, u32[]{:S(2)}) copy-start(bf16[8,512,128]{2,1,0:T(8,128)(2,1)} %copy-done.8) | copy-start | bytes 3145732
  85.3 2.0 %copy-start.11 = (bf16[8,512,128]{2,1,0:T(8,128)(2,1)S(1)}, bf16[8,512,128]{2,1,0:T(8,128)(2,1)}, u32[]{:S(2)}) copy-start(bf16[8,512,128]{2,1,0:T(8,128)(2,1)} %copy-done.10) | copy-start | bytes 3145732
  85.3 2.1 %copy-start.13 = (bf16[8,256,128]{2,1,0:T(8,128)(2,1)S(1)}, bf16[8,256,128]{2,1,0:T(8,128)(2,1)}, u32[]{:S(2)}) copy-start(bf16[8,256,128]{2,1,0:T(8,128)(2,1)} %copy-done.12) | copy-start | bytes 1572868
  115.3 0.8 copy-start.2
  150.2 4.3 %copy-start.16 = (bf16[8,48,512]{2,1,0:T(8,128)(2,1)S(1)}, bf16[8,48,512]{2,1,0:T(8,128)(2,1)}, u32[]{:S(2)}) copy-start(bf16[8,48,512]{2,1,0:T(8,128)(2,1)} %get-tuple-element.21) | copy-start | bytes 1179652
  150.2 4.3 %copy-start.17 = (bf16[384,128]{1,0:T(8,128)(2,1)S(1)}, bf16[384,128]{1,0:T(8,128)(2,1)}, u32[]{:S(2)}) copy-start(bf16[384,128]{1,0:T(8,128)(2,1)} %get-tuple-element.23) | copy-start | bytes 294916
where the time goes:
time: 156 us
  Pallas kernels  114 us (73%)
  matrix products  20.9 us (13%)
  local copies, waits for them, and re-layouts  11.1 us (7%)
  other arithmetic  8.93 us (6%)
    pallas_call x1, Pallas kernels, exchange(): pl.pallas_call(functools.partial(exchange_kernel, counts), in_specs=[whol...  52.8 us
    pallas_call x1, Pallas kernels, gather(): pl.pallas_call(functools.partial(gather_kernel, counts), in_specs=[pl.Blo...  33.3 us
    pallas_call x1, Pallas kernels, attention(): pl.pallas_call(functools.partial(attention_kernel, tp_count), grid=(block...  27.9 us
    unnamed x38, local copies, waits for them, and re-layouts  9.58 us
    dot_general x1, matrix products, body(): jnp.einsum('secf,efd->secd', expert_hidden, expert_down, preferred_elemen...  5.35 us
    dot_general x1, matrix products, body(): jnp.dot(heads_all, weight_cols, preferred_element_type=jnp.float32)  4.32 us
    dot_general x1, matrix products, body(): jnp.dot(shared_hidden, shared_down, preferred_element_type=jnp.float32)  4.25 us

commit v1 on v0

v1 whole, which is shorter than its diff:
```python
import functools
import types

import jax
import jax.numpy as jnp
from jax import lax
from jax.experimental import pallas as pl
from jax.experimental.pallas import tpu as pltpu
from jax.sharding import PartitionSpec as P

EPS_NORM = 1e-06
ROUTED_SCALE = 2.5
LOG2E = 1.4426950408889634
MESH = pl.DeviceIdType.MESH
BF16 = jnp.bfloat16
F32 = jnp.float32
INPUTS = (
    "queries",
    "keys",
    "values",
    "bias",
    "out_w",
    "tokens",
    "gain",
    "ids",
    "scores",
    "sh_gate",
    "sh_up",
    "sh_down",
    "ex_gate",
    "ex_up",
    "ex_down",
)
OUTPUTS = ("mixed", "mix")


def columns(index, width):
    return pl.ds(pl.multiple_of(index * width, width), width)


def dot(left, right):
    return jnp.dot(left, right, preferred_element_type=F32)


class Plan:
    def __init__(self, ep, tp, queries, key_bias, moe_input, route_ids, expert_gate):
        self.ep, self.tp = ep, tp
        self.chips = tp // 2
        self.span = queries[0]
        self.heads = key_bias[1]
        self.size = queries[1] // self.heads
        self.half = ep // 2
        self.groups = self.half // self.heads
        self.share = self.span // self.groups
        self.sub = min(self.share, max(16, self.span // self.half))
        self.subs = self.share // self.sub
        self.width = min(256, self.span)
        self.tokens, self.features = moe_input
        self.col = self.features // tp
        self.topk = route_ids[1]
        self.experts = ep * expert_gate[0]
        capacity = 3 * self.tokens * self.topk // (2 * self.experts)
        self.cap = -(-capacity // 16) * 16
        self.slots = self.experts * self.cap
        self.hidden = expert_gate[2]
        self.rows = self.slots + self.tokens


def kernel(p, names, *refs):
    s = types.SimpleNamespace(**dict(zip(names, refs, strict=True)))
    ep, tp, half, heads, groups = p.ep, p.tp, p.half, p.heads, p.groups
    share, size, span, sub, subs = p.share, p.size, p.span, p.sub, p.subs
    own, own_tp = lax.axis_index("ep"), lax.axis_index("tp")
    side, loc = own // half, lax.rem(own, half)
    own_head, own_group = loc // groups, lax.rem(loc, groups)
    chip, core = own_tp // 2, lax.rem(own_tp, 2)
    beside = own_tp + 1 - 2 * core
    across = [lax.rem(chip + i, p.chips) for i in range(1, p.chips)]

    def remote(source, target, send, recv, axis, device):
        return pltpu.make_async_remote_copy(
            src_ref=source,
            dst_ref=target,
            send_sem=send,
            recv_sem=recv,
            device_id={axis: device},
            device_id_type=MESH,
        )

    def arrived(target, recv):
        remote(target, target, recv, recv, "tp", beside).wait_recv()

    sent = []

    def start(copy):
        copy.start()
        sent.append(copy)

    loads = []

    def load(source, target):
        copy = pltpu.make_async_copy(source, target, s.load.at[len(loads)])
        copy.start()
        loads.append(copy)
        return copy

    in_load = load(s.tokens, s.x_in)
    barrier = pltpu.get_barrier_semaphore()
    for i in range(1, ep):
        pl.semaphore_signal(
            barrier, inc=1, device_id={"ep": lax.rem(own + i, ep)}, device_id_type=MESH
        )
    for i in range(1, tp):
        pl.semaphore_signal(
            barrier, inc=1, device_id={"tp": lax.rem(own_tp + i, tp)}, device_id_type=MESH
        )
    bias = s.bias[...].astype(F32) * LOG2E
    for head in range(heads):
        s.b_stage[head] = jnp.broadcast_to(bias[head : head + 1, :], (8, span))
    index = lax.broadcasted_iota(jnp.int32, (p.width, p.width), 0)
    s.tri[...] = (index > lax.broadcasted_iota(jnp.int32, (p.width, p.width), 1)).astype(F32).astype(BF16)
    with jax.named_scope("enter"):
        pl.semaphore_wait(barrier, ep + tp - 2)

    def part(kind, head):
        if kind == 2:
            return s.b_stage.at[head]
        return (s.keys, s.values)[kind].at[:, columns(head, size)]

    part_outs = (s.k, s.v, s.b)

    def query_part(device):
        return s.queries.at[
            columns(lax.rem(device, groups), share), columns(device // groups, size)
        ]

    near = [lax.rem(loc + i, half) for i in range(1, half)]

    def send_part(kind):
        for other in near:
            start(
                remote(
                    part(kind, other // groups),
                    part_outs[kind].at[loc],
                    s.kv_send.at[kind, other],
                    s.kv_recv.at[kind, loc],
                    "ep",
                    side * half + other,
                )
            )

    kv_own = [
        pltpu.make_async_copy(part(kind, own_head), part_outs[kind].at[loc], s.kv_local.at[kind])
        for kind in range(3)
    ] + [pltpu.make_async_copy(query_part(loc), s.q.at[own], s.kv_local.at[3])]
    for copy in kv_own:
        copy.start()
    loads_shared = [load(s.sh_gate, s.w_sg), load(s.sh_up, s.w_su)]
    loads_expert = [load(s.ex_gate.at[0], s.w_eg), load(s.ex_up.at[0], s.w_eu)]

    with jax.named_scope("norm"):
        in_load.wait()
        inputs = s.x_in[...].astype(F32)
        normed = (
            inputs
            * lax.rsqrt(jnp.mean(inputs * inputs, axis=-1, keepdims=True) + EPS_NORM)
            * s.gain[...]
        ).astype(BF16)
        s.normed[...] = normed
        ids = s.ids[...]
        padded = -(-p.experts // 8) * 8
        expert = lax.broadcasted_iota(jnp.int32, (padded, p.tokens), 0)
        chosen = [(expert == ids[k : k + 1, :]).astype(F32) for k in range(p.topk)]
        named = chosen[0]
        for k in range(1, p.topk):
            named = named + chosen[k]
        before = (
            lax.broadcasted_iota(jnp.int32, (p.tokens, p.tokens), 0)
            < lax.broadcasted_iota(jnp.int32, (p.tokens, p.tokens), 1)
        ).astype(F32).astype(BF16)
        earlier = dot(named.astype(BF16), before)
        slot_row = lax.broadcasted_iota(jnp.int32, (p.slots, p.tokens), 0)
        slot_ids = []
        for k in range(p.topk):
            place = jnp.sum(chosen[k] * earlier, axis=0, keepdims=True).astype(jnp.int32)
            slot_ids.append(ids[k : k + 1, :] * p.cap + place)

        def table(weights):
            total = jnp.zeros((p.slots, p.tokens), F32)
            for k in range(p.topk):
                total = jnp.where(slot_row == slot_ids[k], weights[k], total)
            return total

        per = p.slots // ep
        ones = jnp.ones((1, p.tokens), F32)
        own_cols = s.normed[:, columns(own_tp, p.col)]
        outgoing = dot(table([ones] * p.topk).astype(BF16), own_cols).astype(BF16)
        s.rows_stage[...] = outgoing.reshape(ep, per, p.col)

    def grid_rows(device, slot):
        return s.grid.at[columns(device, per), columns(slot, p.col)]

    s.grid[columns(own, per), columns(own_tp, p.col)] = s.rows_stage[own]
    for i in range(1, ep):
        other = lax.rem(own + i, ep)
        start(
            remote(
                s.rows_stage.at[other],
                grid_rows(own, own_tp),
                s.rows_send.at[other],
                s.rows_recv.at[own],
                "ep",
                other,
            )
        )

    def far_query(device, piece, target):
        rows = pl.ds(lax.rem(target, groups) * share + piece * sub, sub)
        return remote(
            s.queries.at[rows, columns(target // groups, size)],
            s.q.at[half + device, pl.ds(piece * sub, sub)],
            s.q_send.at[half + target, piece],
            s.q_recv.at[half + device, piece],
            "ep",
            target,
        )

    def send_far(piece):
        @pl.when(side == 1)
        def _():
            for i in range(half):
                far_query(loc, piece, lax.rem(loc + i, half)).start()

    for kind in range(3):
        send_part(kind)
    send_far(0)
    for other in near:
        start(
            remote(
                query_part(other),
                s.q.at[own],
                s.q_send.at[other, 0],
                s.q_recv.at[loc, 0],
                "ep",
                side * half + other,
            )
        )
    for piece in range(1, subs):
        send_far(piece)

    def weight_pieces(number, source, target):
        for y in range(p.chips):
            load(source.at[:, columns(y * 2 + core, p.col)], target.at[core, y])
            start(
                remote(
                    source.at[:, columns(y * 2 + 1 - core, p.col)],
                    target.at[core, y],
                    s.w_send.at[number, y],
                    s.w_recv.at[number, y],
                    "tp",
                    beside,
                )
            )

    down_from = len(loads)
    weight_pieces(0, s.ex_down.at[0], s.w_ed)
    weight_pieces(1, s.sh_down, s.w_sd)
    weight_pieces(2, s.out_w, s.w_o)
    loads_down = loads[down_from:]

    tile = min(256, p.hidden)

    def gated(source, gate, up, first, count):
        def step(n, _):
            at = columns(n, tile)
            rows_in = source[...]
            left = dot(rows_in, gate[:, at])
            right = dot(rows_in, up[:, at])
            value = left / (1.0 + jnp.exp(-left)) * right
            s.hid[core, pl.ds(first, count), at] = value.astype(BF16)
            return 0

        lax.fori_loop(0, p.hidden // tile, step, 0)

    def swap_hidden(first, count, number):
        at = s.hid.at[core, pl.ds(first, count)]
        start(remote(at, at, s.hid_send.at[number], s.hid_recv.at[number], "tp", beside))

    with jax.named_scope("shared"):
        for copy in loads_shared:
            copy.wait()
        gated(s.normed, s.w_sg, s.w_su, p.slots, p.tokens)
        swap_hidden(p.slots, p.tokens, 1)

    sources = [lax.rem(own + ep - i, ep) for i in range(ep)]
    with jax.named_scope("rows_wait"):
        for source in sources:
            mine = grid_rows(source, own_tp)
            if source is not sources[0]:
                arrived(mine, s.rows_recv.at[source])
            for other in [y * 2 + core for y in across] + [beside]:
                start(
                    remote(
                        mine,
                        mine,
                        s.relay_send.at[source, other],
                        s.relay_recv.at[source, own_tp],
                        "tp",
                        other,
                    )
                )
    with jax.named_scope("relay_wait"):
        for source in sources:
            for y in across:
                slot = y * 2 + core
                piece = grid_rows(source, slot)
                arrived(piece, s.relay_recv.at[source, slot])
                start(
                    remote(
                        piece,
                        piece,
                        s.pass_send.at[source, slot],
                        s.relay_recv.at[source, slot],
                        "tp",
                        beside,
                    )
                )
        for source in sources:
            for y in [chip] + across:
                slot = y * 2 + 1 - core
                arrived(grid_rows(source, slot), s.relay_recv.at[source, slot])

    with jax.named_scope("expert"):
        for copy in loads_expert:
            copy.wait()
        gated(s.grid, s.w_eg, s.w_eu, 0, p.slots)
        swap_hidden(0, p.slots, 0)
    with jax.named_scope("swap_wait"):
        for copy in loads_down:
            copy.wait()
        for number, target in enumerate((s.w_ed, s.w_sd, s.w_o)):
            for y in range(p.chips):
                arrived(target.at[1 - core, y], s.w_recv.at[number, y])
        arrived(s.hid.at[1 - core, pl.ds(p.slots, p.tokens)], s.hid_recv.at[1])
        arrived(s.hid.at[1 - core, pl.ds(0, p.slots)], s.hid_recv.at[0])

    def down(y):
        routed = dot(s.hid[0, : p.slots], s.w_ed[0, y]) + dot(s.hid[1, : p.slots], s.w_ed[1, y])
        common = dot(s.hid[0, p.slots :], s.w_sd[0, y]) + dot(s.hid[1, p.slots :], s.w_sd[1, y])
        return routed, common

    with jax.named_scope("down"):
        for y in across:
            routed, common = down(y)
            s.part_send[y, : p.slots] = routed.astype(BF16)
            s.part_send[y, p.slots :] = common.astype(BF16)
            start(
                remote(
                    s.part_send.at[y],
                    s.part_recv.at[chip],
                    s.part_ssem.at[y],
                    s.part_rsem.at[chip],
                    "tp",
                    y * 2 + core,
                )
            )
        routed, common = down(chip)
        s.part_own[: p.slots] = routed
        s.part_own[p.slots :] = common

    scale = size ** (-0.5) * LOG2E

    def unit(query, block, carry, masked):
        count = query.shape[0]
        total, passed = carry
        key, value, bias_of = s.k[block], s.v[block], s.b[block]
        for first in range(span - p.width, -1, -p.width):
            logit = (
                lax.dot_general(
                    query,
                    key[first : first + p.width],
                    (((1,), (1,)), ((), ())),
                    preferred_element_type=F32,
                )
                * scale
                + bias_of[0:1, first : first + p.width]
            )
            drop = jnp.maximum(logit, jnp.log2(1.0 + jnp.exp2(jnp.minimum(logit, 126.0))))
            base = logit - drop
            if masked:
                shape = (count, p.width)
                visible = first + lax.broadcasted_iota(
                    jnp.int32, shape, 1
                ) < own_group * share + lax.broadcasted_iota(jnp.int32, shape, 0)
                drop = jnp.where(visible, drop, 0.0)
            later = dot(drop.astype(BF16), s.tri[...])
            weight = jnp.exp2(base - later - passed)
            if masked:
                weight = jnp.where(visible, weight, 0.0)
            passed = passed + later[:, 0:1] + drop[:, 0:1]
            total = total + dot(weight.astype(BF16), value[first : first + p.width])
        return total, passed

    def zeros(count):
        return jnp.zeros((count, size), F32), jnp.zeros((count, 1), F32)

    def heads_rows(piece, group):
        return pl.ds(pl.multiple_of((piece * groups + group) * sub, sub), sub)

    def out_piece(block, piece):
        return remote(
            s.o_stage.at[block, pl.ds(piece * sub, sub)],
            s.heads.at[core, heads_rows(piece, own_group), columns(own_head, size)],
            s.o_send.at[block, piece],
            s.o_recv.at[loc, piece],
            "ep",
            side * half + block,
        )

    def hand_on(block, piece):
        @pl.when(block != loc)
        def _():
            out_piece(block, piece).start()

        @pl.when(block == loc)
        def _():
            s.heads[core, heads_rows(piece, own_group), columns(own_head, size)] = s.o_stage[
                block, pl.ds(piece * sub, sub)
            ]

    def local_block(block, _):
        with jax.named_scope("q_wait"):

            @pl.when(block != loc)
            def _():
                arrived(s.q.at[side * half + block], s.q_recv.at[block, 0])

        with jax.named_scope("local"):
            query = s.q[side * half + block]
            carry = unit(query, block, zeros(share), True)
            carry = lax.fori_loop(
                0, block, lambda i, c: unit(query, block - 1 - i, c, False), carry
            )

        @pl.when(side == 0)
        def _():
            s.o_stage[block] = carry[0].astype(BF16)
            for piece in range(subs):
                hand_on(block, piece)

        @pl.when(side == 1)
        def _():
            s.o_part[block] = carry[0]
            s.passed[block] = jnp.broadcast_to(jnp.exp2(-carry[1]), (share, size))

        return 0

    with jax.named_scope("kv_wait"):
        for copy in kv_own:
            copy.wait()
        for block in range(half):

            @pl.when(block != loc)
            def _():
                for kind in range(3):
                    arrived(part_outs[kind].at[block], s.kv_recv.at[kind, block])


    def back_copy(other):
        return remote(
            s.back_stage.at[other],
            s.back.at[own],
            s.back_send.at[other],
            s.back_recv.at[own],
            "ep",
            other,
        )

    def give_back():
        with jax.named_scope("sums"):
            total = s.part_own[...]
            for y in across:
                arrived(s.part_recv.at[y], s.part_rsem.at[y])
                total = total + s.part_recv[y].astype(F32)
            s.part_own[...] = total
            s.back_stage[...] = total[: p.slots].astype(BF16).reshape(ep, per, p.col)
            s.back[own] = s.back_stage[own]
            for i in range(1, ep):
                other = lax.rem(own + i, ep)
                back_copy(other).start()

    def combine():
        with jax.named_scope("back_wait"):
            for i in range(1, ep):
                other = lax.rem(own + i, ep)
                arrived(s.back.at[other], s.back_recv.at[other])
        with jax.named_scope("combine"):
            scores = s.scores[...]
            score_sum = scores[0:1, :]
            for k in range(1, p.topk):
                score_sum = score_sum + scores[k : k + 1, :]
            gates = table(
                [scores[k : k + 1, :] / score_sum * ROUTED_SCALE for k in range(p.topk)]
            ).T
            high = gates.astype(BF16)
            low = (gates - high.astype(F32)).astype(BF16)
            returned = s.back[...].reshape(p.slots, p.col)
            s.mix[...] = (s.part_own[p.slots :] + dot(high, returned) + dot(low, returned)).astype(BF16)

    def out_rows(piece, count):
        return pl.ds(piece * groups * sub, count * groups * sub)

    def sibling(piece, count, slot):
        at = s.heads.at[slot, out_rows(piece, count)]
        return remote(at, at, s.sib_send.at[piece], s.sib_recv.at[piece], "tp", beside)

    def out_copy(y, piece, count):
        at = out_rows(piece, count)
        return remote(
            s.out_send.at[y, at],
            s.out_recv.at[chip, at],
            s.out_ssem.at[y, piece],
            s.out_rsem.at[chip, piece],
            "tp",
            y * 2 + core,
        )

    def project(piece, count):
        with jax.named_scope("o_wait"):
            for number in range(piece, piece + count):
                for source in range(half):

                    @pl.when(source != loc)
                    def _():
                        group, head = source % groups, source // groups
                        arrived(
                            s.heads.at[
                                core,
                                heads_rows(number, group),
                                pl.ds(head * size, size),
                            ],
                            s.o_recv.at[source, number],
                        )

        with jax.named_scope("sib_wait"):
            sibling(piece, count, core).start()
            sibling(piece, count, 1 - core).wait_recv()
        at = out_rows(piece, count)
        with jax.named_scope("proj"):
            for y in across:
                s.out_send[y, at] = (
                    dot(s.heads[0, at], s.w_o[0, y]) + dot(s.heads[1, at], s.w_o[1, y])
                ).astype(BF16)
                out_copy(y, piece, count).start()
            s.out_own[at] = dot(s.heads[0, at], s.w_o[0, chip]) + dot(s.heads[1, at], s.w_o[1, chip])

    def finish(piece, count):
        at = out_rows(piece, count)
        total = s.out_own[at]
        with jax.named_scope("out_wait"):
            for y in across:
                arrived(s.out_recv.at[y, at], s.out_rsem.at[y, piece])
                total = total + s.out_recv[y, at].astype(F32)
        total = total.astype(BF16)
        for number in range(piece, piece + count):
            for group in range(groups):
                first = ((number - piece) * groups + group) * sub
                s.mixed[pl.ds(group * share + number * sub, sub)] = total[first : first + sub]
        for y in across:
            out_copy(y, piece, count).wait_send()
        sibling(piece, count, core).wait_send()

    def mirror(piece):
        return remote(
            s.hl_stage.at[piece],
            s.hl.at[piece],
            s.hl_send.at[piece],
            s.hl_recv.at[piece],
            "ep",
            loc + half,
        )

    @pl.when(side == 0)
    def _():
        def far_tile(piece):
            with jax.named_scope("far_wait"):
                for block in range(half):
                    target = s.q.at[half + block, pl.ds(piece * sub, sub)]
                    arrived(target, s.q_recv.at[half + block, piece])
            with jax.named_scope("far"):
                query = s.q[half:, piece * sub : (piece + 1) * sub].reshape(half * sub, size)
                carry = lax.fori_loop(
                    0, half, lambda i, c: unit(query, half - 1 - i, c, False), zeros(half * sub)
                )
            s.hl_stage[piece] = carry[0].astype(BF16)
            mirror(piece).start()

        for piece in range(subs):
            far_tile(piece)
        give_back()
        lax.fori_loop(0, half, local_block, 0)
        project(0, subs)
        combine()
        finish(0, subs)
        for piece in range(subs):
            mirror(piece).wait_send()

    @pl.when(side == 1)
    def _():
        def merge(piece):
            with jax.named_scope("hl_wait"):
                arrived(s.hl.at[piece], s.hl_recv.at[piece])
            rows = slice(piece * sub, (piece + 1) * sub)
            s.o_stage[:, rows] = (
                s.o_part[:, rows]
                + s.passed[:, rows] * s.hl[piece].astype(F32).reshape(half, sub, size)
            ).astype(BF16)
            for block in range(half):
                hand_on(block, piece)

        lax.fori_loop(0, half, local_block, 0)
        give_back()
        merge(0)
        for piece in range(1, subs):
            merge(piece)
            project(piece - 1, 1)
        project(subs - 1, 1)
        for piece in range(subs - 1):
            finish(piece, 1)
        combine()
        finish(subs - 1, 1)
        for piece in range(subs):
            for i in range(half):
                far_query(loc, piece, lax.rem(loc + i, half)).wait_send()

    for i in range(1, ep):
        back_copy(lax.rem(own + i, ep)).wait_send()
    for block in range(half):

        @pl.when(block != loc)
        def _():
            for piece in range(subs):
                out_piece(block, piece).wait_send()

    for copy in sent:
        copy.wait_send()


def fused(p, *operands):
    dma = pltpu.SemaphoreType.DMA
    ep, tp, half, chips = p.ep, p.tp, p.half, p.chips
    per = p.slots // ep
    vmem = pl.BlockSpec(memory_space=pltpu.VMEM)
    free = pl.BlockSpec(memory_space=pl.ANY)
    small = ("bias", "gain", "ids", "scores")

    def buffer(shape, kind=BF16):
        return pltpu.VMEM(shape, kind)

    depth = p.heads * p.size
    scratch = {
        "q": buffer((ep, p.share, p.size)),
        "k": buffer((half, p.span, p.size)),
        "v": buffer((half, p.span, p.size)),
        "b": buffer((half, 8, p.span), F32),
        "b_stage": buffer((p.heads, 8, p.span), F32),
        "tri": buffer((p.width, p.width)),
        "hl_stage": buffer((p.subs, half * p.sub, p.size)),
        "hl": buffer((p.subs, half * p.sub, p.size)),
        "o_part": buffer((half, p.share, p.size), F32),
        "passed": buffer((half, p.share, p.size), F32),
        "o_stage": buffer((half, p.share, p.size)),
        "heads": buffer((2, p.span, depth)),
        "normed": buffer((p.tokens, p.features)),
        "rows_stage": buffer((ep, per, p.col)),
        "grid": buffer((p.slots, p.features)),
        "x_in": buffer((p.tokens, p.features)),
        "w_sg": buffer((p.features, p.hidden)),
        "w_su": buffer((p.features, p.hidden)),
        "w_eg": buffer((p.features, p.hidden)),
        "w_eu": buffer((p.features, p.hidden)),
        "w_sd": buffer((2, chips, p.hidden, p.col)),
        "w_ed": buffer((2, chips, p.hidden, p.col)),
        "w_o": buffer((2, chips, depth, p.col)),
        "hid": buffer((2, p.rows, p.hidden)),
        "part_send": buffer((chips, p.rows, p.col)),
        "part_recv": buffer((chips, p.rows, p.col)),
        "part_own": buffer((p.rows, p.col), F32),
        "back_stage": buffer((ep, per, p.col)),
        "back": buffer((ep, per, p.col)),
        "out_send": buffer((chips, p.span, p.col)),
        "out_recv": buffer((chips, p.span, p.col)),
        "out_own": buffer((p.span, p.col), F32),
        "load": dma((5 + 3 * chips,)),
        "kv_local": dma((4,)),
        "kv_send": dma((3, half)),
        "kv_recv": dma((3, half)),
        "q_send": dma((ep, p.subs)),
        "q_recv": dma((ep, p.subs)),
        "hl_send": dma((p.subs,)),
        "hl_recv": dma((p.subs,)),
        "o_send": dma((half, p.subs)),
        "o_recv": dma((half, p.subs)),
        "sib_send": dma((p.subs,)),
        "sib_recv": dma((p.subs,)),
        "w_send": dma((3, chips)),
        "w_recv": dma((3, chips)),
        "rows_send": dma((ep,)),
        "rows_recv": dma((ep,)),
        "relay_send": dma((ep, tp)),
        "relay_recv": dma((ep, tp)),
        "pass_send": dma((ep, tp)),
        "hid_send": dma((2,)),
        "hid_recv": dma((2,)),
        "part_ssem": dma((chips,)),
        "part_rsem": dma((chips,)),
        "back_send": dma((ep,)),
        "back_recv": dma((ep,)),
        "out_ssem": dma((chips, p.subs)),
        "out_rsem": dma((chips, p.subs)),
    }
    names = INPUTS + OUTPUTS + tuple(scratch)
    return pl.pallas_call(
        functools.partial(kernel, p, names),
        in_specs=[vmem if name in small else free for name in INPUTS],
        out_specs=[vmem, vmem],
        out_shape=[
            jax.ShapeDtypeStruct((p.span, p.col), BF16),
            jax.ShapeDtypeStruct((p.tokens, p.col), BF16),
        ],
        scratch_shapes=list(scratch.values()),
        compiler_params=pltpu.CompilerParams(
            collective_id=0, has_side_effects=True, vmem_limit_bytes=62 * 1024 * 1024
        ),
        name="fused",
    )(*operands)


def body(
    queries,
    keys,
    values,
    key_bias,
    out_weight,
    moe_input,
    moe_gain,
    route_ids,
    route_scores,
    shared_gate,
    shared_up,
    shared_down,
    expert_gate,
    expert_up,
    expert_down,
):
    p = Plan(
        lax.axis_size("ep"),
        lax.axis_size("tp"),
        queries.shape,
        key_bias.shape,
        moe_input.shape,
        route_ids.shape,
        expert_gate.shape,
    )
    return fused(
        p,
        queries,
        keys,
        values,
        key_bias.T,
        out_weight,
        moe_input,
        moe_gain.reshape(1, -1),
        route_ids.T,
        route_scores.T,
        shared_gate,
        shared_up,
        shared_down,
        expert_gate,
        expert_up,
        expert_down,
    )


def solution(mesh):
    return jax.shard_map(
        body,
        mesh=mesh,
        in_specs=(
            P("ep", "tp"),
            P("ep", "tp"),
            P("ep", "tp"),
            P("ep", "tp"),
            P("tp", None),
            P("ep", None),
            P(),
            P("ep", None),
            P("ep", None),
            P(None, "tp"),
            P(None, "tp"),
            P("tp", None),
            P("ep", None, "tp"),
            P("ep", None, "tp"),
            P("ep", "tp", None),
        ),
        out_specs=(P("ep", "tp"), P("ep", "tp")),
        check_vma=False,
    )
```

time: 156 us -> 86.1 us (0.55)
  the two profiles are of different devices: /device:TPU:31 before, /device:TPU:11 now
where the time goes in v1:
time: 86.1 us; the launch traced here: 85.8 us
  Pallas kernels  81.7 us (95%)
  local copies, waits for them, and re-layouts  3.44 us (4%)
    pallas_call x1, Pallas kernels, fused(): pl.pallas_call(functools.partial(kernel, p, names), in_specs=[vmem if nam...  81.7 us
    unnamed x2, local copies, waits for them, and re-layouts  3.44 us

profile of v1, /device:TPU:11, one launch (start us, length us, event | category | flops | bytes accessed | tf_op | source)
XLA Modules:
  0.0 85.8 jit_solution(6186762223432692651)
XLA Ops:
  0.6 81.7 %fused.1 = (bf16[512,512]{1,0:T(8,128)(2,1)}, bf16[128,512]{1,0:T(8,128)(2,1)}) custom-call(bf16[512,512]{1,0:T(8,128)(2,1)} %refs_0_.1, bf16[512,512]{1,0:T(8,128)(2,1)} %refs_1_.1, bf16[512,512]{1,0:T(8,128)(2,1)} %refs_2_.1, bf16[4,512]{1,0:T(4,128)(2,1)} %bitcast.5, bf16[512,2048]{1,0:T(8,128)(2,1)} %refs_4_.1, bf16[128,2048]{1,0:T(8,128)(2,1)} %refs_5_.1, ...), custom_call_target="tpu_custom_call" | custom-call | tf_op jit(solution)/shard_map/fused/pallas_call | solution.py:723
  82.4 1.9 %copy.19 = bf16[512,512]{1,0:T(8,128)(2,1)} copy(bf16[512,512]{1,0:T(8,128)(2,1)} %get-tuple-element.4) | data formatting | bytes 1048576
  84.3 1.6 %copy.20 = bf16[128,512]{1,0:T(8,128)(2,1)} copy(bf16[128,512]{1,0:T(8,128)(2,1)} %get-tuple-element.5) | data formatting | bytes 262144

commit v2 on v1

--- a/solution.py
+++ b/solution.py
@@ -231,22 +231,26 @@
             for i in range(half):
                 far_query(loc, piece, lax.rem(loc + i, half)).start()
 
+    row = max(1, half // 2)
+
+    def send_queries(same_row):
+        for other in near:
+
+            @pl.when((other // row == loc // row) == same_row)
+            def _():
+                remote(
+                    query_part(other),
+                    s.q.at[own],
+                    s.q_send.at[other, 0],
+                    s.q_recv.at[loc, 0],
+                    "ep",
+                    side * half + other,
+                ).start()
+
+    send_far(0)
     for kind in range(3):
         send_part(kind)
-    send_far(0)
-    for other in near:
-        start(
-            remote(
-                query_part(other),
-                s.q.at[own],
-                s.q_send.at[other, 0],
-                s.q_recv.at[loc, 0],
-                "ep",
-                side * half + other,
-            )
-        )
-    for piece in range(1, subs):
-        send_far(piece)
+    send_queries(True)
 
     def weight_pieces(number, source, target):
         for y in range(p.chips):
@@ -330,6 +334,13 @@
                 slot = y * 2 + 1 - core
                 arrived(grid_rows(source, slot), s.relay_recv.at[source, slot])
 
+    for piece in range(1, min(3, subs)):
+        send_far(piece)
+
+    @pl.when(side == 1)
+    def _():
+        send_queries(False)
+
     with jax.named_scope("expert"):
         for copy in loads_expert:
             copy.wait()
@@ -367,6 +378,13 @@
         routed, common = down(chip)
         s.part_own[: p.slots] = routed
         s.part_own[p.slots :] = common
+
+    for piece in range(3, subs):
+        send_far(piece)
+
+    @pl.when(side == 0)
+    def _():
+        send_queries(False)
 
     scale = size ** (-0.5) * LOG2E
 
@@ -455,16 +473,19 @@
 
         return 0
 
-    with jax.named_scope("kv_wait"):
-        for copy in kv_own:
-            copy.wait()
-        for block in range(half):
-
-            @pl.when(block != loc)
-            def _():
-                for kind in range(3):
-                    arrived(part_outs[kind].at[block], s.kv_recv.at[kind, block])
-
+    def keys_arrive(blocks):
+        with jax.named_scope("kv_wait"):
+            for block in blocks:
+
+                @pl.when(block == loc)
+                def _():
+                    for copy in kv_own:
+                        copy.wait()
+
+                @pl.when(block != loc)
+                def _():
+                    for kind in range(3):
+                        arrived(part_outs[kind].at[block], s.kv_recv.at[kind, block])
 
     def back_copy(other):
         return remote(
@@ -595,10 +616,17 @@
             s.hl_stage[piece] = carry[0].astype(BF16)
             mirror(piece).start()
 
-        for piece in range(subs):
+        first = jnp.where(loc < row, row, 0)
+        keys_arrive(range(row))
+        lax.fori_loop(0, first, local_block, 0)
+        keys_arrive(range(row, half))
+        ahead = max(1, subs // 2)
+        for piece in range(ahead):
+            far_tile(piece)
+        lax.fori_loop(first, half, local_block, 0)
+        for piece in range(ahead, subs):
             far_tile(piece)
         give_back()
-        lax.fori_loop(0, half, local_block, 0)
         project(0, subs)
         combine()
         finish(0, subs)
@@ -618,6 +646,7 @@
             for block in range(half):
                 hand_on(block, piece)
 
+        keys_arrive(range(half))
         lax.fori_loop(0, half, local_block, 0)
         give_back()
         merge(0)
@@ -642,6 +671,15 @@
             for piece in range(subs):
                 out_piece(block, piece).wait_send()
 
+    for other in near:
+        remote(
+            query_part(other),
+            s.q.at[own],
+            s.q_send.at[other, 0],
+            s.q_recv.at[loc, 0],
+            "ep",
+            side * half + other,
+        ).wait_send()
     for copy in sent:
         copy.wait_send()
 
@@ -736,6 +774,22 @@
     )(*operands)
 
 
+def settle_kernel(mixed_in, mix_in, mixed_out, mix_out):
+    mixed_out[...] = mixed_in[...]
+    mix_out[...] = mix_in[...]
+
+
+def settle(mixed, mix):
+    vmem = pl.BlockSpec(memory_space=pltpu.VMEM)
+    return pl.pallas_call(
+        settle_kernel,
+        in_specs=[vmem, vmem],
+        out_specs=[vmem, vmem],
+        out_shape=[jax.ShapeDtypeStruct(x.shape, x.dtype) for x in (mixed, mix)],
+        name="settle",
+    )(mixed, mix)
+
+
 def body(
     queries,
     keys,
@@ -762,7 +816,7 @@
         route_ids.shape,
         expert_gate.shape,
     )
-    return fused(
+    mixed, mix = fused(
         p,
         queries,
         keys,
@@ -780,6 +834,7 @@
         expert_up,
         expert_down,
     )
+    return settle(mixed, mix)
 
 
 def solution(mesh):

time: 86.1 us -> 81.1 us (0.942)
  the two profiles are of different devices: /device:TPU:11 before, /device:TPU:31 now
where the time goes in v2:
time: 81.1 us; the launch traced here: 79.8 us
  Pallas kernels  79.1 us (98%)
    pallas_call x1, Pallas kernels, fused(): pl.pallas_call(functools.partial(kernel, p, names), in_specs=[vmem if nam...  77.2 us
    pallas_call x1, Pallas kernels, settle(): pl.pallas_call(settle_kernel, in_specs=[vmem, vmem], out_specs=[vmem, vme...  1.93 us

profile of v2, /device:TPU:31, one launch (start us, length us, event | category | flops | bytes accessed | tf_op | source)
XLA Modules:
  0.0 79.8 jit_solution(2462824202170302053)
XLA Ops:
  0.6 77.2 %fused.1 = (bf16[512,512]{1,0:T(8,128)(2,1)}, bf16[128,512]{1,0:T(8,128)(2,1)}) custom-call(bf16[512,512]{1,0:T(8,128)(2,1)} %refs_0_.1, bf16[512,512]{1,0:T(8,128)(2,1)} %refs_1_.1, bf16[512,512]{1,0:T(8,128)(2,1)} %refs_2_.1, bf16[4,512]{1,0:T(4,128)(2,1)} %bitcast.5, bf16[512,2048]{1,0:T(8,128)(2,1)} %refs_4_.1, bf16[128,2048]{1,0:T(8,128)(2,1)} %refs_5_.1, ...), custom_call_target="tpu_custom_call" | custom-call | tf_op jit(solution)/shard_map/fused/pallas_call | solution.py:761
  77.8 1.9 %settle.1 = (bf16[512,512]{1,0:T(8,128)(2,1)}, bf16[128,512]{1,0:T(8,128)(2,1)}) custom-call(bf16[512,512]{1,0:T(8,128)(2,1)} %get-tuple-element.4.mixed_in, bf16[128,512]{1,0:T(8,128)(2,1)} %get-tuple-element.5.mix_in), custom_call_target="tpu_custom_call" | custom-call | tf_op jit(solution)/shard_map/settle/pallas_call | solution.py:784

commit v3 on v2

--- a/solution.py
+++ b/solution.py
@@ -334,12 +334,10 @@
                 slot = y * 2 + 1 - core
                 arrived(grid_rows(source, slot), s.relay_recv.at[source, slot])
 
-    for piece in range(1, min(3, subs)):
-        send_far(piece)
-
-    @pl.when(side == 1)
-    def _():
-        send_queries(False)
+    if subs > 1:
+        send_far(1)
+
+    send_queries(False)
 
     with jax.named_scope("expert"):
         for copy in loads_expert:
@@ -378,13 +376,6 @@
         routed, common = down(chip)
         s.part_own[: p.slots] = routed
         s.part_own[p.slots :] = common
-
-    for piece in range(3, subs):
-        send_far(piece)
-
-    @pl.when(side == 0)
-    def _():
-        send_queries(False)
 
     scale = size ** (-0.5) * LOG2E
 
@@ -601,6 +592,28 @@
             loc + half,
         )
 
+    def drain():
+        for i in range(1, ep):
+            back_copy(lax.rem(own + i, ep)).wait_send()
+        for block in range(half):
+
+            @pl.when(block != loc)
+            def _():
+                for piece in range(subs):
+                    out_piece(block, piece).wait_send()
+
+        for other in near:
+            remote(
+                query_part(other),
+                s.q.at[own],
+                s.q_send.at[other, 0],
+                s.q_recv.at[loc, 0],
+                "ep",
+                side * half + other,
+            ).wait_send()
+        for copy in sent:
+            copy.wait_send()
+
     @pl.when(side == 0)
     def _():
         def far_tile(piece):
@@ -629,9 +642,10 @@
         give_back()
         project(0, subs)
         combine()
-        finish(0, subs)
         for piece in range(subs):
             mirror(piece).wait_send()
+        drain()
+        finish(0, subs)
 
     @pl.when(side == 1)
     def _():
@@ -647,6 +661,9 @@
                 hand_on(block, piece)
 
         keys_arrive(range(half))
+        for piece in range(2, subs):
+            for i in range(half):
+                far_query(loc, piece, lax.rem(loc + i, half)).start()
         lax.fori_loop(0, half, local_block, 0)
         give_back()
         merge(0)
@@ -657,31 +674,11 @@
         for piece in range(subs - 1):
             finish(piece, 1)
         combine()
-        finish(subs - 1, 1)
         for piece in range(subs):
             for i in range(half):
                 far_query(loc, piece, lax.rem(loc + i, half)).wait_send()
-
-    for i in range(1, ep):
-        back_copy(lax.rem(own + i, ep)).wait_send()
-    for block in range(half):
-
-        @pl.when(block != loc)
-        def _():
-            for piece in range(subs):
-                out_piece(block, piece).wait_send()
-
-    for other in near:
-        remote(
-            query_part(other),
-            s.q.at[own],
-            s.q_send.at[other, 0],
-            s.q_recv.at[loc, 0],
-            "ep",
-            side * half + other,
-        ).wait_send()
-    for copy in sent:
-        copy.wait_send()
+        drain()
+        finish(subs - 1, 1)
 
 
 def fused(p, *operands):

time: 81.1 us -> 80.2 us (0.989)
  the two profiles are of different devices: /device:TPU:31 before, /device:TPU:19 now
where the time goes in v3:
time: 80.2 us; the launch traced here: 80 us
  Pallas kernels  79.3 us (99%)
    pallas_call x1, Pallas kernels, fused(): pl.pallas_call(functools.partial(kernel, p, names), in_specs=[vmem if nam...  77.4 us
    pallas_call x1, Pallas kernels, settle(): pl.pallas_call(settle_kernel, in_specs=[vmem, vmem], out_specs=[vmem, vme...  1.93 us

profile of v3, /device:TPU:19, one launch (start us, length us, event | category | flops | bytes accessed | tf_op | source)
XLA Modules:
  0.0 80.0 jit_solution(16448196914188413482)
XLA Ops:
  0.6 77.4 %fused.1 = (bf16[512,512]{1,0:T(8,128)(2,1)}, bf16[128,512]{1,0:T(8,128)(2,1)}) custom-call(bf16[512,512]{1,0:T(8,128)(2,1)} %refs_0_.1, bf16[512,512]{1,0:T(8,128)(2,1)} %refs_1_.1, bf16[512,512]{1,0:T(8,128)(2,1)} %refs_2_.1, bf16[4,512]{1,0:T(4,128)(2,1)} %bitcast.5, bf16[512,2048]{1,0:T(8,128)(2,1)} %refs_4_.1, bf16[128,2048]{1,0:T(8,128)(2,1)} %refs_5_.1, ...), custom_call_target="tpu_custom_call" | custom-call | tf_op jit(solution)/shard_map/fused/pallas_call | solution.py:758
  78.1 1.9 %settle.1 = (bf16[512,512]{1,0:T(8,128)(2,1)}, bf16[128,512]{1,0:T(8,128)(2,1)}) custom-call(bf16[512,512]{1,0:T(8,128)(2,1)} %get-tuple-element.4.mixed_in, bf16[128,512]{1,0:T(8,128)(2,1)} %get-tuple-element.5.mix_in), custom_call_target="tpu_custom_call" | custom-call | tf_op jit(solution)/shard_map/settle/pallas_call | solution.py:781
